TPU v7x, 32 devices: a whole 2x2x4 slice. The times are simulated.
32 devices in a mesh: ep: 4 (over y, x), tp: 8 (over z, core).
Axes of the slice: x: 2, y: 2, z: 4, core: 2. Of those that a mesh axis runs over, the one named last changes fastest.
Arguments:
- tokens: bfloat16 [128, 4096], P('ep', 'tp'), may hold values from -16 to 16
- routing: int32 [128, 4], P('ep'), may hold values from 0 to 7, all different within a row; in each aligned block of 32 rows (0 to 31, 32 to 63, ...) at most 32 rows name the same one
- gate_weights: float32 [128, 4], P('ep'), may hold values from 0.1 to 1
- w_gate: bfloat16 [8, 1024, 4096], P('ep', 'tp'), may hold values from -0.09375 to 0.09375
- w_up: bfloat16 [8, 1024, 4096], P('ep', 'tp'), may hold values from -0.09375 to 0.09375
- w_down: bfloat16 [8, 1024, 4096], P('ep', None, 'tp'), may hold values from -2 to 2
- out_gain: float32 [4096], P('tp'), may hold values from 0.1 to 1.9
Outputs:
- mixed: bfloat16 [128, 4096], P('ep', 'tp')
Inputs may be any that keep to these rules, and one draw needn't show every extreme that they name: `routing`: in each aligned block of 32 rows (the tokens of one index of ep) no expert is named by more than 32 entries, and in every draw some expert is named by exactly 32 entries of some block. The 4 entries of a row differ.
All inputs are finite; a program needn't handle non-finite values.
Results may differ from a plain program's by a relative error of at most 0.0057.
Values may be sent and summed in bfloat16 or wider, within the bound.
A program may use at most 64 MiB of HBM per device.

v0:
```python
import jax
import jax.numpy as jnp
from jax import lax
from jax.sharding import PartitionSpec as P

D = 4096
TOPK = 4
EXP_DEV = 2
norm_eps = 1e-05


def body(tokens, routing, gate_weights, w_gate, w_up, w_down, out_gain):
    ep_count = lax.axis_size("ep")
    tok_rows = tokens.shape[0]
    width_part = tokens.shape[1]
    experts = EXP_DEV * ep_count
    slot_count = 2 * tok_rows * TOPK // experts
    span_rows = ep_count * slot_count
    total_slots = EXP_DEV * span_rows
    flat_route = routing.reshape(-1)
    expert_ids = jnp.arange(experts, dtype=jnp.int32)
    hit_table = (flat_route[:, None] == expert_ids[None, :]).astype(jnp.int32)
    running = jnp.cumsum(hit_table, axis=0) - hit_table
    slot_rank = jnp.sum(running * hit_table, axis=1)
    slot_target = flat_route % EXP_DEV * span_rows + flat_route // EXP_DEV * slot_count + slot_rank
    entry_targets = slot_target.reshape(tok_rows, TOPK)
    slot_ids = jnp.arange(total_slots, dtype=jnp.int32)
    select_table = jnp.any(entry_targets[None, :, :] == slot_ids[:, None, None], axis=2).astype(
        jnp.bfloat16
    )
    outgoing = jnp.dot(select_table, tokens, preferred_element_type=jnp.float32).astype(
        jnp.bfloat16
    )
    outgoing = outgoing.reshape(EXP_DEV, ep_count, slot_count, width_part)
    arrived = lax.all_to_all(outgoing, "ep", split_axis=1, concat_axis=1, tiled=True).reshape(
        EXP_DEV, span_rows, width_part
    )
    piece_cols = lax.all_gather(arrived, "tp", axis=2, tiled=True)
    gate_sum = jnp.einsum("efn,esn->efs", w_gate, piece_cols, preferred_element_type=jnp.float32)
    up_sum = jnp.einsum("efn,esn->efs", w_up, piece_cols, preferred_element_type=jnp.float32)
    square_sum = jnp.einsum(
        "esn,esn->es", piece_cols, piece_cols, preferred_element_type=jnp.float32
    )
    row_scale = lax.rsqrt(square_sum / D + norm_eps)[:, None, :]
    hidden = (jax.nn.silu(gate_sum * row_scale) * (up_sum * row_scale)).astype(jnp.bfloat16)
    out_part = w_down.shape[2]
    expert_out = jnp.einsum(
        "ens,end->esd",
        lax.all_gather(hidden, "tp", axis=1, tiled=True),
        w_down,
        preferred_element_type=jnp.float32,
    ).astype(jnp.bfloat16)
    returned = lax.all_to_all(
        expert_out.reshape(EXP_DEV, ep_count, slot_count, out_part),
        "ep",
        split_axis=1,
        concat_axis=1,
        tiled=True,
    )
    returned = returned.reshape(total_slots, out_part)
    chosen = returned[slot_target].astype(jnp.float32).reshape(tok_rows, TOPK, out_part)
    combined = jnp.sum(chosen * gate_weights[:, :, None], axis=1)
    square_total = lax.psum(jnp.sum(combined * combined, axis=1), "tp")
    final_scale = lax.rsqrt(square_total / D + norm_eps)
    return (combined * final_scale[:, None] * out_gain[None, :]).astype(jnp.bfloat16)


def solution(mesh):
    placed = (
        P("ep", "tp"),
        P("ep", None),
        P("ep", None),
        P("ep", "tp", None),
        P("ep", "tp", None),
        P("ep", None, "tp"),
        P("tp"),
    )
    return jax.shard_map(body, mesh=mesh, in_specs=placed, out_specs=P("ep", "tp"), check_vma=False)
```

profile of v0, /device:TPU:0, one launch (start us, length us, event | category | flops | bytes accessed | tf_op | source)
XLA Modules:
  0.0 102.4 jit_solution(12375172439346588443)
XLA Ops:
  6.5 0.9 copy.33
  7.5 0.1 eq.30
  7.6 0.1 fusion.6
  7.7 0.2 reduce_window_sum.11
  7.8 0.2 select_reduce_fusion
  8.0 0.1 reduce_sum.32
  8.1 0.1 copy.38
  8.2 0.1 fusion.5
  8.3 1.0 convolution_convert_fusion
  9.4 10.7 %all_to_all.10 = bf16[2,4,32,512]{3,2,0,1:T(8,128)(2,1)S(1)} all-to-all(bf16[2,4,32,512]{3,2,0,1:T(8,128)(2,1)S(1)} %copy.39), channel_id=1, replica_groups=mesh['ep'=4,'tp'=8] {'ep'}, dimensions={1} | all-to-all | bytes 524288 | tf_op jit(solution)/shard_map/all_to_all | solution.py:35
  20.1 0.7 copy.40
  20.8 0.0 all-gather.2.cloned.1.call-update
  20.9 0.1 reshape.182
  21.0 28.9 %all-gather.2.cloned.1.call-done = bf16[2,128,4096]{2,1,0:T(8,128)(2,1)} async-done(((bf16[2,128,512]{2,1,0:T(8,128)(2,1)}), bf16[2,128,4096]{2,1,0:T(8,128)(2,1)}) %all-gather.2.cloned.1.call-update) | async-done | bytes 2097168 | tf_op jit(solution)/shard_map/all_gather | solution.py:38
  49.9 2.2 %fusion = f32[2,128]{1,0:T(2,128)S(1)} fusion(bf16[2,128,4096]{2,1,0:T(8,128)(2,1)} %all-gather.2.cloned.1.call-done), kind=kLoop, calls=%fused_computation.2 | loop fusion | flops 3145472 | bytes 2098176 | tf_op jit(solution)/shard_map/esn,esn->es/dot_general | solution.py:41
  52.1 0.0 copy-start.4
  52.2 2.5 %fusion.3 = f32[2,128,128]{1,2,0:T(8,128)S(1)} fusion(bf16[2,128,4096]{2,1,0:T(8,128)(2,1)S(1)} %copy-done.1, bf16[2,128,4096]{2,1,0:T(8,128)(2,1)} %param.10, f32[2,128]{1,0:T(2,128)S(1)} %add_rsqrt_fusion), kind=kOutput, calls=%fused_computation.9 | convolution fusion | flops 268468224 | bytes 4326400 | tf_op jit(solution)/shard_map/efn,esn->efs/dot_general | solution.py:39
  54.6 0.7 fusion.4
  55.3 13.9 %all_gather.7 = bf16[2,1024,128]{1,2,0:T(8,128)(2,1)S(1)} all-gather(bf16[2,128,128]{1,2,0:T(8,128)(2,1)S(1)} %fusion.4), channel_id=1, replica_groups=mesh['ep'=4,'tp'=8] {'tp'}, dimensions={1}, use_global_device_ids=true | all-gather | bytes 589824 | tf_op jit(solution)/shard_map/all_gather | solution.py:49
  69.2 0.4 convolution_convert_fusion.1
  69.7 0.0 copy-start.3
  69.7 0.7 copy.41
  70.4 3.6 %all-to-all-start.1 = ((bf16[2,4,32,512]{3,2,0,1:T(8,128)(2,1)}), bf16[2,4,32,512]{3,2,0,1:T(8,128)(2,1)S(1)}, u32[]{:S(2)}, u32[]{:S(2)}) async-start(bf16[2,4,32,512]{3,2,0,1:T(8,128)(2,1)} %copy.41), calls=%async_computation.1 | async-start | bytes 524288 | tf_op jit(solution)/shard_map/all_to_all | solution.py:53
  74.1 0.0 copy-done.2
  74.1 0.1 copy.44
  74.2 5.8 %all-to-all-done.1 = bf16[2,4,32,512]{3,2,0,1:T(8,128)(2,1)S(1)} async-done(((bf16[2,4,32,512]{3,2,0,1:T(8,128)(2,1)}), bf16[2,4,32,512]{3,2,0,1:T(8,128)(2,1)S(1)}, u32[]{:S(2)}, u32[]{:S(2)}) %all-to-all-start.1) | async-done | bytes 262176 | tf_op jit(solution)/shard_map/all_to_all | solution.py:53
  80.0 0.8 gather_fusion
  80.8 0.1 reshape.183
  80.9 0.2 multiply_reduce_fusion
  81.1 0.1 multiply_reduce_fusion.1
  81.2 13.6 %psum.7 = f32[32]{0:T(128)S(1)} all-reduce(f32[32]{0:T(128)S(1)} %multiply_reduce_fusion.1), channel_id=1, replica_groups=mesh['ep'=4,'tp'=8] {'tp'}, use_global_device_ids=true, to_apply=%region_5.6 | all-reduce | flops 32 | bytes 256 | tf_op jit(solution)/shard_map/psum | solution.py:63
  94.8 0.7 multiply_convert_fusion
  (15 shorter events, 0.1 us)
Async XLA Ops:
  6.5 62.7 %copy-start = (bf16[2,1024,512]{2,1,0:T(8,128)(2,1)S(1)}, bf16[2,1024,512]{2,1,0:T(8,128)(2,1)}, u32[]{:S(2)}) copy-start(bf16[2,1024,512]{2,1,0:T(8,128)(2,1)} %param.12) | copy-start | bytes 6291460
  6.5 43.4 %all-gather.2.cloned.1.call-start = ((), (), s32[]{:S(2)}) async-start(), calls=%async_computation.2 | async-start | bytes 2359296 | tf_op jit(solution)/shard_map/all_gather | solution.py:38
  49.9 2.2 %copy-start.1 = (bf16[2,128,4096]{2,1,0:T(8,128)(2,1)S(1)}, bf16[2,128,4096]{2,1,0:T(8,128)(2,1)}, u32[]{:S(2)}) copy-start(bf16[2,128,4096]{2,1,0:T(8,128)(2,1)} %all-gather.2.cloned.1.call-done) | copy-start | bytes 6291460
  52.1 2.5 %copy-start.4 = (bf16[2,128,4096]{2,1,0:T(8,128)(2,1)S(1)}, bf16[2,128,4096]{2,1,0:T(8,128)(2,1)}, u32[]{:S(2)}) copy-start(bf16[2,128,4096]{2,1,0:T(8,128)(2,1)} %param.11) | copy-start | bytes 6291460
  69.2 4.8 %copy-start.2 = (f32[32,4]{0,1:T(4,128)S(1)}, f32[32,4]{0,1:T(4,128)}, u32[]{:S(2)}) copy-start(f32[32,4]{0,1:T(4,128)} %param.9) | copy-start | bytes 1540
  69.7 25.2 %copy-start.3 = (f32[512]{0:T(512)S(1)}, f32[512]{0:T(512)}, u32[]{:S(2)}) copy-start(f32[512]{0:T(512)} %param.13) | copy-start | bytes 6148
  70.4 9.5 %all-to-all-start.1 = ((bf16[2,4,32,512]{3,2,0,1:T(8,128)(2,1)}), bf16[2,4,32,512]{3,2,0,1:T(8,128)(2,1)S(1)}, u32[]{:S(2)}, u32[]{:S(2)}) async-start(bf16[2,4,32,512]{3,2,0,1:T(8,128)(2,1)} %copy.41), calls=%async_computation.1 | async-start | bytes 524288 | tf_op jit(solution)/shard_map/all_to_all | solution.py:53
Sparse Core Ops, SparseCore 0:
  21.0 28.8 all-gather.1
where the time goes:
time: 103 us; the launch traced here: 102 us
  blocking collectives  38.2 us (37%)
  waiting for transfers between devices  34.7 us (34%)
  between operations  13.5 us (13%)
  matrix products  4.63 us (4%)
  other arithmetic  3.86 us (4%)
  local copies, waits for them, and re-layouts  3.84 us (4%)
  starting transfers between devices  3.65 us (4%)
    all_gather x1, waiting for transfers between devices, body(): piece_cols = lax.all_gather(arrived, 'tp', axis=2, tiled=True)  28.9 us
    all_gather x1, blocking collectives, body(): lax.all_gather(hidden, 'tp', axis=1, tiled=True)  13.9 us
    psum x1, blocking collectives, body(): square_total = lax.psum(jnp.sum(combined * combined, axis=1), 'tp')  13.6 us
    all_to_all x1, blocking collectives, body(): lax.all_to_all(outgoing, 'ep', split_axis=1, concat_axis=1, tiled=True)  10.7 us
    all_to_all x1, waiting for transfers between devices, body(): lax.all_to_all(expert_out.reshape(EXP_DEV, ep_count, slot_count, out_part...  5.77 us
    all_to_all x1, starting transfers between devices, body(): lax.all_to_all(expert_out.reshape(EXP_DEV, ep_count, slot_count, out_part...  3.65 us
    dot_general x1, matrix products, body(): jnp.einsum('efn,esn->efs', w_gate, piece_cols, preferred_element_type=jnp...  2.45 us
    dot_general x1, other arithmetic, body(): jnp.einsum('esn,esn->es', piece_cols, piece_cols, preferred_element_type=...  2.23 us
  transfers between devices with their start and end apart: 2, of which 2 were waited for; matrix products, arithmetic and copies ran while one was open for 0% of the time, Pallas kernels for 0%

commit v1 on v0

--- a/solution.py
+++ b/solution.py
@@ -7,6 +7,22 @@
 TOPK = 4
 EXP_DEV = 2
 norm_eps = 1e-05
+
+
+def product_in_turn(x, axis, dim, term):
+    devices, mine, width = (lax.axis_size(axis), lax.axis_index(axis), x.shape[dim])
+    right = [(i, (i + 1) % devices) for i in range(devices)]
+    left = [(i, (i - 1) % devices) for i in range(devices)]
+    half = devices // 2
+    from_left = from_right = x
+    total = term(x, mine * width)
+    for step in range(1, half + 1):
+        from_left = lax.ppermute(from_left, axis, right)
+        if step < devices - half:
+            from_right = lax.ppermute(from_right, axis, left)
+            total = total + term(from_right, (mine + step) % devices * width)
+        total = total + term(from_left, (mine - step) % devices * width)
+    return total
 
 
 def body(tokens, routing, gate_weights, w_gate, w_up, w_down, out_gain):
@@ -44,11 +60,16 @@
     row_scale = lax.rsqrt(square_sum / D + norm_eps)[:, None, :]
     hidden = (jax.nn.silu(gate_sum * row_scale) * (up_sum * row_scale)).astype(jnp.bfloat16)
     out_part = w_down.shape[2]
-    expert_out = jnp.einsum(
-        "ens,end->esd",
-        lax.all_gather(hidden, "tp", axis=1, tiled=True),
-        w_down,
-        preferred_element_type=jnp.float32,
+    expert_out = product_in_turn(
+        hidden,
+        "tp",
+        1,
+        lambda part, start: jnp.einsum(
+            "ens,end->esd",
+            part,
+            lax.dynamic_slice_in_dim(w_down, start, part.shape[1], axis=1),
+            preferred_element_type=jnp.float32,
+        ),
     ).astype(jnp.bfloat16)
     returned = lax.all_to_all(
         expert_out.reshape(EXP_DEV, ep_count, slot_count, out_part),

time: 103 us -> 110 us (1.068)
  blocking collectives: 38.2 us -> 24.3 us
  starting transfers between devices: 3.65 us -> 14.4 us
  waiting for transfers between devices: 34.7 us -> 44.1 us
  matrix products: 4.63 us -> 5.88 us
    all_gather x1 -> x0, blocking collectives: 13.9 us -> none  [body(): lax.all_gather(hidden, 'tp', axis=1, tiled=True)]
    ppermute x0 -> x7, starting transfers between devices: none -> 10.7 us  [the longest x3 10.4 us: product_in_turn(): from_right = lax.ppermute(from_right, axis, left)]
    ppermute x0 -> x7, waiting for transfers between devices: none -> 10.1 us  [the longest x4 10.1 us: product_in_turn(): from_left = lax.ppermute(from_left, axis, right)]
    dot_general x1 -> x8, matrix products: 0.45 us -> 1.7 us  [body(): jnp.einsum('ens,end->esd', part, lax.dynamic_slice_in_dim(w_down, start,...]
  transfers between devices with their start and end apart: 2 -> 9, of which waited for: 2 -> 6; matrix products, arithmetic and copies ran while one was open for 0% -> 2% of each run, Pallas kernels for 0% -> 0%
where the time goes in v1:
time: 110 us
  waiting for transfers between devices  44.1 us (40%)
  blocking collectives  24.3 us (22%)
  starting transfers between devices  14.4 us (13%)
  between operations  13.8 us (13%)
  matrix products  5.88 us (5%)
  other arithmetic  3.86 us (4%)
  local copies, waits for them, and re-layouts  3.84 us (3%)
    all_gather x1, waiting for transfers between devices, body(): piece_cols = lax.all_gather(arrived, 'tp', axis=2, tiled=True)  28.8 us
    psum x1, blocking collectives, body(): square_total = lax.psum(jnp.sum(combined * combined, axis=1), 'tp')  13.6 us
    all_to_all x1, blocking collectives, body(): lax.all_to_all(outgoing, 'ep', split_axis=1, concat_axis=1, tiled=True)  10.7 us
    ppermute x3, starting transfers between devices, product_in_turn(): from_right = lax.ppermute(from_right, axis, left)  10.4 us
    ppermute x4, waiting for transfers between devices, product_in_turn(): from_left = lax.ppermute(from_left, axis, right)  10.1 us
    all_to_all x1, waiting for transfers between devices, body(): lax.all_to_all(expert_out.reshape(EXP_DEV, ep_count, slot_count, out_part...  5.25 us
    all_to_all x1, starting transfers between devices, body(): lax.all_to_all(expert_out.reshape(EXP_DEV, ep_count, slot_count, out_part...  3.65 us
    dot_general x1, matrix products, body(): jnp.einsum('efn,esn->efs', w_gate, piece_cols, preferred_element_type=jnp...  2.45 us
  transfers between devices with their start and end apart: 9, of which 6 were waited for; matrix products, arithmetic and copies ran while one was open for 2% of the time, Pallas kernels for 0%

profile of v1, /device:TPU:0, one launch (start us, length us, event | category | flops | bytes accessed | tf_op | source)
XLA Modules:
  0.0 110.2 jit_solution(17483547740056711763)
XLA Ops:
  6.5 0.9 copy.33
  7.7 0.2 reduce_window_sum.11
  8.3 1.0 convolution_convert_fusion
  9.4 10.7 %all_to_all.10 = bf16[2,4,32,512]{3,2,0,1:T(8,128)(2,1)S(1)} all-to-all(bf16[2,4,32,512]{3,2,0,1:T(8,128)(2,1)S(1)} %copy.39), channel_id=1, replica_groups=mesh['ep'=4,'tp'=8] {'ep'}, dimensions={1} | all-to-all | bytes 524288 | tf_op jit(solution)/shard_map/all_to_all | solution.py:51
  20.1 0.7 copy.40
  21.1 28.8 %all-gather.2.cloned.1.call-done = bf16[2,128,4096]{2,1,0:T(8,128)(2,1)} async-done(((bf16[2,128,512]{2,1,0:T(8,128)(2,1)}), bf16[2,128,4096]{2,1,0:T(8,128)(2,1)}) %all-gather.2.cloned.1.call-update) | async-done | bytes 2097168 | tf_op jit(solution)/shard_map/all_gather | solution.py:54
  49.9 2.2 %fusion = f32[2,128]{1,0:T(2,128)S(1)} fusion(bf16[2,128,4096]{2,1,0:T(8,128)(2,1)} %all-gather.2.cloned.1.call-done), kind=kLoop, calls=%fused_computation.2 | loop fusion | flops 3145472 | bytes 2098176 | tf_op jit(solution)/shard_map/esn,esn->es/dot_general | solution.py:57
  52.2 2.5 %fusion.6 = f32[2,128,128]{1,2,0:T(8,128)S(1)} fusion(bf16[2,128,4096]{2,1,0:T(8,128)(2,1)S(1)} %copy-done.1, bf16[2,128,4096]{2,1,0:T(8,128)(2,1)} %param.10, f32[2,128]{1,0:T(2,128)S(1)} %add_rsqrt_fusion), kind=kOutput, calls=%fused_computation.16 | convolution fusion | flops 268468224 | bytes 4326400 | tf_op jit(solution)/shard_map/efn,esn->efs/dot_general | solution.py:55
  54.6 0.7 fusion.7
  55.3 0.3 collective-permute-start.1
  55.6 3.3 %collective-permute-start = (bf16[2,128,128]{1,2,0:T(8,128)(2,1)S(1)}, bf16[2,128,128]{1,2,0:T(8,128)(2,1)S(1)}, u32[]{:S(2)}, u32[]{:S(2)}) collective-permute-start(bf16[2,128,128]{1,2,0:T(8,128)(2,1)S(1)} %fusion.7), channel_id=1, source_target_pairs={{0,7},{1,0},{2,1},{3,2},{4,3},{5,4},{6,5},{7,6},{8,15},{9,8},{10,9... | collective-permute-start | bytes 196616 | tf_op jit(solution)/shard_map/ppermute | solution.py:22
  58.9 0.2 fusion.17
  59.2 2.1 %collective-permute-done.1 = bf16[2,128,128]{1,2,0:T(8,128)(2,1)S(1)} collective-permute-done((bf16[2,128,128]{1,2,0:T(8,128)(2,1)S(1)}, bf16[2,128,128]{1,2,0:T(8,128)(2,1)S(1)}, u32[]{:S(2)}, u32[]{:S(2)}) %collective-permute-start.1) | collective-permute-done | bytes 65568 | tf_op jit(solution)/shard_map/ppermute | solution.py:20
  61.3 3.5 %collective-permute-start.2 = (bf16[2,128,128]{1,2,0:T(8,128)(2,1)S(1)}, bf16[2,128,128]{1,2,0:T(8,128)(2,1)S(1)}, u32[]{:S(2)}, u32[]{:S(2)}) collective-permute-start(bf16[2,128,128]{1,2,0:T(8,128)(2,1)S(1)} %collective-permute-done), channel_id=1, source_target_pairs={{0,7},{1,0},{2,1},{3,2},{4,3},{5,4},{6,5},{7,6},{8,15},{9,8},{10,9... | collective-permute-start | bytes 196616 | tf_op jit(solution)/shard_map/ppermute | solution.py:22
  64.8 0.2 convolution_add_fusion.4
  65.0 0.2 convolution_add_fusion.3
  65.3 1.5 %collective-permute-done.3 = bf16[2,128,128]{1,2,0:T(8,128)(2,1)S(1)} collective-permute-done((bf16[2,128,128]{1,2,0:T(8,128)(2,1)S(1)}, bf16[2,128,128]{1,2,0:T(8,128)(2,1)S(1)}, u32[]{:S(2)}, u32[]{:S(2)}) %collective-permute-start.3) | collective-permute-done | bytes 65568 | tf_op jit(solution)/shard_map/ppermute | solution.py:20
  66.8 0.2 fusion.12
  67.0 3.6 %collective-permute-start.4 = (bf16[2,128,128]{1,2,0:T(8,128)(2,1)S(1)}, bf16[2,128,128]{1,2,0:T(8,128)(2,1)S(1)}, u32[]{:S(2)}, u32[]{:S(2)}) collective-permute-start(bf16[2,128,128]{1,2,0:T(8,128)(2,1)S(1)} %collective-permute-done.2), channel_id=1, source_target_pairs={{0,7},{1,0},{2,1},{3,2},{4,3},{5,4},{6,5},{7,6},{8,15},{9,8},{10,9... | collective-permute-start | bytes 196616 | tf_op jit(solution)/shard_map/ppermute | solution.py:22
  70.6 0.2 fusion.2
  70.8 1.5 %collective-permute-done.5 = bf16[2,128,128]{1,2,0:T(8,128)(2,1)S(1)} collective-permute-done((bf16[2,128,128]{1,2,0:T(8,128)(2,1)S(1)}, bf16[2,128,128]{1,2,0:T(8,128)(2,1)S(1)}, u32[]{:S(2)}, u32[]{:S(2)}) %collective-permute-start.5) | collective-permute-done | bytes 65568 | tf_op jit(solution)/shard_map/ppermute | solution.py:20
  72.3 0.2 fusion.9
  72.5 0.2 fusion.1
  72.7 5.0 %collective-permute-done.6 = bf16[2,128,128]{1,2,0:T(8,128)(2,1)S(1)} collective-permute-done((bf16[2,128,128]{1,2,0:T(8,128)(2,1)S(1)}, bf16[2,128,128]{1,2,0:T(8,128)(2,1)S(1)}, u32[]{:S(2)}, u32[]{:S(2)}) %collective-permute-start.6) | collective-permute-done | bytes 65568 | tf_op jit(solution)/shard_map/ppermute | solution.py:20
  77.7 0.2 fusion.3
  78.0 0.7 copy.41
  78.7 3.6 %all-to-all-start.1 = ((bf16[2,4,32,512]{3,2,0,1:T(8,128)(2,1)}), bf16[2,4,32,512]{3,2,0,1:T(8,128)(2,1)S(1)}, u32[]{:S(2)}, u32[]{:S(2)}) async-start(bf16[2,4,32,512]{3,2,0,1:T(8,128)(2,1)} %copy.41), calls=%async_computation.1 | async-start | bytes 524288 | tf_op jit(solution)/shard_map/all_to_all | solution.py:74
  82.4 5.3 %all-to-all-done.1 = bf16[2,4,32,512]{3,2,0,1:T(8,128)(2,1)S(1)} async-done(((bf16[2,4,32,512]{3,2,0,1:T(8,128)(2,1)}), bf16[2,4,32,512]{3,2,0,1:T(8,128)(2,1)S(1)}, u32[]{:S(2)}, u32[]{:S(2)}) %all-to-all-start.1) | async-done | bytes 262176 | tf_op jit(solution)/shard_map/all_to_all | solution.py:74
  87.7 0.8 gather_fusion
  88.7 0.2 multiply_reduce_fusion
  89.0 13.6 %psum.7 = f32[32]{0:T(128)S(1)} all-reduce(f32[32]{0:T(128)S(1)} %multiply_reduce_fusion.1), channel_id=1, replica_groups=mesh['ep'=4,'tp'=8] {'tp'}, use_global_device_ids=true, to_apply=%region_5.6 | all-reduce | flops 32 | bytes 256 | tf_op jit(solution)/shard_map/psum | solution.py:84
  102.6 0.7 multiply_convert_fusion
  (35 shorter events, 1.2 us)
Async XLA Ops:
  6.5 52.4 %copy-start = (bf16[2,1024,512]{2,1,0:T(8,128)(2,1)S(1)}, bf16[2,1024,512]{2,1,0:T(8,128)(2,1)}, u32[]{:S(2)}) copy-start(bf16[2,1024,512]{2,1,0:T(8,128)(2,1)} %param.12) | copy-start | bytes 6291460
  6.5 43.4 %all-gather.2.cloned.1.call-start = ((), (), s32[]{:S(2)}) async-start(), calls=%async_computation.2 | async-start | bytes 2359296 | tf_op jit(solution)/shard_map/all_gather | solution.py:54
  49.9 2.2 %copy-start.1 = (bf16[2,128,4096]{2,1,0:T(8,128)(2,1)S(1)}, bf16[2,128,4096]{2,1,0:T(8,128)(2,1)}, u32[]{:S(2)}) copy-start(bf16[2,128,4096]{2,1,0:T(8,128)(2,1)} %all-gather.2.cloned.1.call-done) | copy-start | bytes 6291460
  52.1 2.5 %copy-start.4 = (bf16[2,128,4096]{2,1,0:T(8,128)(2,1)S(1)}, bf16[2,128,4096]{2,1,0:T(8,128)(2,1)}, u32[]{:S(2)}) copy-start(bf16[2,128,4096]{2,1,0:T(8,128)(2,1)} %param.11) | copy-start | bytes 6291460
  55.3 5.9 %collective-permute-start.1 = (bf16[2,128,128]{1,2,0:T(8,128)(2,1)S(1)}, bf16[2,128,128]{1,2,0:T(8,128)(2,1)S(1)}, u32[]{:S(2)}, u32[]{:S(2)}) collective-permute-start(bf16[2,128,128]{1,2,0:T(8,128)(2,1)S(1)} %fusion.7), channel_id=1, source_target_pairs={{0,1},{1,2},{2,3},{3,4},{4,5},{5,6},{6,7},{7,0},{8,9},{9,10},{10,1... | collective-permute-start | bytes 196616 | tf_op jit(solution)/shard_map/ppermute | solution.py:20
  55.6 5.7 %collective-permute-start = (bf16[2,128,128]{1,2,0:T(8,128)(2,1)S(1)}, bf16[2,128,128]{1,2,0:T(8,128)(2,1)S(1)}, u32[]{:S(2)}, u32[]{:S(2)}) collective-permute-start(bf16[2,128,128]{1,2,0:T(8,128)(2,1)S(1)} %fusion.7), channel_id=1, source_target_pairs={{0,7},{1,0},{2,1},{3,2},{4,3},{5,4},{6,5},{7,6},{8,15},{9,8},{10,9... | collective-permute-start | bytes 196616 | tf_op jit(solution)/shard_map/ppermute | solution.py:22
  61.3 5.5 %collective-permute-start.3 = (bf16[2,128,128]{1,2,0:T(8,128)(2,1)S(1)}, bf16[2,128,128]{1,2,0:T(8,128)(2,1)S(1)}, u32[]{:S(2)}, u32[]{:S(2)}) collective-permute-start(bf16[2,128,128]{1,2,0:T(8,128)(2,1)S(1)} %collective-permute-done.1), channel_id=1, source_target_pairs={{0,1},{1,2},{2,3},{3,4},{4,5},{5,6},{6,7},{7,0},{8,9},{9,10},{10,1... | collective-permute-start | bytes 196616 | tf_op jit(solution)/shard_map/ppermute | solution.py:20
  61.3 5.7 %collective-permute-start.2 = (bf16[2,128,128]{1,2,0:T(8,128)(2,1)S(1)}, bf16[2,128,128]{1,2,0:T(8,128)(2,1)S(1)}, u32[]{:S(2)}, u32[]{:S(2)}) collective-permute-start(bf16[2,128,128]{1,2,0:T(8,128)(2,1)S(1)} %collective-permute-done), channel_id=1, source_target_pairs={{0,7},{1,0},{2,1},{3,2},{4,3},{5,4},{6,5},{7,6},{8,15},{9,8},{10,9... | collective-permute-start | bytes 196616 | tf_op jit(solution)/shard_map/ppermute | solution.py:22
  66.8 5.5 %collective-permute-start.5 = (bf16[2,128,128]{1,2,0:T(8,128)(2,1)S(1)}, bf16[2,128,128]{1,2,0:T(8,128)(2,1)S(1)}, u32[]{:S(2)}, u32[]{:S(2)}) collective-permute-start(bf16[2,128,128]{1,2,0:T(8,128)(2,1)S(1)} %collective-permute-done.3), channel_id=1, source_target_pairs={{0,1},{1,2},{2,3},{3,4},{4,5},{5,6},{6,7},{7,0},{8,9},{9,10},{10,1... | collective-permute-start | bytes 196616 | tf_op jit(solution)/shard_map/ppermute | solution.py:20
  67.0 5.5 %collective-permute-start.4 = (bf16[2,128,128]{1,2,0:T(8,128)(2,1)S(1)}, bf16[2,128,128]{1,2,0:T(8,128)(2,1)S(1)}, u32[]{:S(2)}, u32[]{:S(2)}) collective-permute-start(bf16[2,128,128]{1,2,0:T(8,128)(2,1)S(1)} %collective-permute-done.2), channel_id=1, source_target_pairs={{0,7},{1,0},{2,1},{3,2},{4,3},{5,4},{6,5},{7,6},{8,15},{9,8},{10,9... | collective-permute-start | bytes 196616 | tf_op jit(solution)/shard_map/ppermute | solution.py:22
  72.3 5.5 %collective-permute-start.6 = (bf16[2,128,128]{1,2,0:T(8,128)(2,1)S(1)}, bf16[2,128,128]{1,2,0:T(8,128)(2,1)S(1)}, u32[]{:S(2)}, u32[]{:S(2)}) collective-permute-start(bf16[2,128,128]{1,2,0:T(8,128)(2,1)S(1)} %collective-permute-done.5), channel_id=1, source_target_pairs={{0,1},{1,2},{2,3},{3,4},{4,5},{5,6},{6,7},{7,0},{8,9},{9,10},{10,1... | collective-permute-start | bytes 196616 | tf_op jit(solution)/shard_map/ppermute | solution.py:20
  72.5 9.9 %copy-start.2 = (f32[32,4]{0,1:T(4,128)S(1)}, f32[32,4]{0,1:T(4,128)}, u32[]{:S(2)}) copy-start(f32[32,4]{0,1:T(4,128)} %param.9) | copy-start | bytes 1540
  72.7 29.9 %copy-start.3 = (f32[512]{0:T(512)S(1)}, f32[512]{0:T(512)}, u32[]{:S(2)}) copy-start(f32[512]{0:T(512)} %param.13) | copy-start | bytes 6148
  78.7 9.0 %all-to-all-start.1 = ((bf16[2,4,32,512]{3,2,0,1:T(8,128)(2,1)}), bf16[2,4,32,512]{3,2,0,1:T(8,128)(2,1)S(1)}, u32[]{:S(2)}, u32[]{:S(2)}) async-start(bf16[2,4,32,512]{3,2,0,1:T(8,128)(2,1)} %copy.41), calls=%async_computation.1 | async-start | bytes 524288 | tf_op jit(solution)/shard_map/all_to_all | solution.py:74
Sparse Core Ops, SparseCore 0:
  21.0 28.8 all-gather.1
